TPU v7x, 32 devices: a whole 2x2x4 slice. The times are simulated.
32 devices in a mesh: sp: 8 (over z, x), tp: 4 (over y, core).
Axes of the slice: x: 2, y: 2, z: 4, core: 2. Of those that a mesh axis runs over, the one named last changes fastest.
Arguments:
- queries: bfloat16 [1024, 2048], P('sp', 'tp'), may hold values from -18 to 90
- projected_key_rows: bfloat16 [1024, 1024], P('sp', 'tp'), may hold values from -18 to 90
- projected_value_rows: bfloat16 [1024, 1024], P('sp', 'tp'), may hold values from -6 to 6
- query_gain: float32 [64], replicated, may hold values from 1 to 6
- key_norm_gain: float32 [64], replicated, may hold values from 1 to 6
- residual: bfloat16 [1024, 2048], P('sp', 'tp'), may hold values from -54 to 54
- out_weight: bfloat16 [2048, 2048], P('tp'), may hold values from -1 to 1
- norm_gain: float32 [2048], P('tp'), may hold values from 0.28 to 4.68
- expert_ids: int32 [1024, 2], P('sp'), may hold values from 0 to 7, as said below
- route_weights: float32 [1024, 2], P('sp'), may hold values from 0.2 to 1
- gate_weight: bfloat16 [8, 2048, 4096], P('sp', None, 'tp'), may hold values from -0.125 to 0.125
- up_weight: bfloat16 [8, 2048, 4096], P('sp', None, 'tp'), may hold values from -0.125 to 0.125
- down_weight: bfloat16 [8, 4096, 2048], P('sp', 'tp'), may hold values from -0.25 to 0.25
- final_gain: float32 [2048], P('tp'), may hold values from 0.1 to 1.9
Outputs:
- layer_out: bfloat16 [1024, 2048], P('sp', 'tp')
Inputs may be any that keep to these rules, and one draw needn't show every extreme that they name: `expert_ids`: each row names two different experts of one group, the group of expert e being e // 4. In every aligned block of 128 rows each group is named by the same number of rows, no expert is named by more than 64 rows, one expert of every group is named by exactly 64 rows, and one expert is named by 64 rows of every block.
All inputs are finite; a program needn't handle non-finite values.
Results may differ from a plain program's by a relative error of at most 0.019.
The roundings to bfloat16 on the way count: a program that leaves them out, or rounds other values in their place, can miss the bound.
Values may be sent and summed in bfloat16 or wider, within the bound.
A program may use at most 64 MiB of HBM per device.

v0:
```python
from functools import reduce
import jax
import jax.numpy as jnp
from jax import lax
from jax.sharding import PartitionSpec as P

D = 2048
HEAD_DIM = 64
GRID_W = 64
TOPK = 2
theta_base = 10000.0
norm_epsilon = 1e-06
residual_scale = 8.0**0.25
far_below = -1e30


def rope_line(halves, angles):
    pair_count = angles.shape[-1]
    first_half = halves[..., :pair_count]
    second_half = halves[..., pair_count:]
    cosine = jnp.cos(angles)[:, None, :]
    sine_part = jnp.sin(angles)[:, None, :]
    return jnp.concatenate(
        [
            first_half * cosine - second_half * sine_part,
            first_half * sine_part + second_half * cosine,
        ],
        -1,
    )


def rotary_over_grid(rows_by_head, token_positions):
    head_size = rows_by_head.shape[-1]
    frequency = theta_base ** (
        -jnp.arange(0, head_size // 2, 2, dtype=jnp.float32) / (head_size // 2)
    )
    grid_row = (token_positions // GRID_W).astype(jnp.float32)
    grid_col = (token_positions % GRID_W).astype(jnp.float32)
    row_part = rope_line(
        rows_by_head[..., : head_size // 2], grid_row[:, None] * frequency[None, :]
    )
    col_part = rope_line(
        rows_by_head[..., head_size // 2 :], grid_col[:, None] * frequency[None, :]
    )
    return jnp.concatenate([row_part, col_part], -1)


def normalize_heads(token_rows, gain_row, head_count):
    shaped = token_rows.astype(jnp.float32).reshape(token_rows.shape[0], head_count, -1)
    scaled = shaped * lax.rsqrt(jnp.mean(shaped * shaped, -1, keepdims=True) + norm_epsilon)
    return scaled * gain_row[None, None, :]


def norm_features(feature_rows, gain_row, feature_total):
    row_sums = jnp.sum(feature_rows, 0)
    squares = jnp.sum(feature_rows * feature_rows, 0)
    row_sums, squares = lax.psum((row_sums, squares), "tp")
    center = row_sums / feature_total
    spread = squares / feature_total - center * center
    return (
        (feature_rows - center[None, :])
        * lax.rsqrt(spread + norm_epsilon)[None, :]
        * gain_row[:, None]
    )


def per_device(
    queries,
    projected_key_rows,
    projected_value_rows,
    query_gain,
    key_norm_gain,
    residual,
    out_weight,
    norm_gain,
    expert_ids,
    route_weights,
    gate_weight,
    up_weight,
    down_weight,
    final_gain,
):
    token_count = queries.shape[0]
    query_heads = queries.shape[1] // HEAD_DIM
    key_heads = projected_key_rows.shape[1] // HEAD_DIM
    queries_per_group = query_heads // key_heads
    token_positions = lax.axis_index("sp") * token_count + jnp.arange(token_count, dtype=jnp.int32)
    queries_after_rotation = rotary_over_grid(
        normalize_heads(queries, query_gain, query_heads), token_positions
    ).astype(jnp.bfloat16)
    keys_after_rotation = rotary_over_grid(
        normalize_heads(projected_key_rows, key_norm_gain, key_heads), token_positions
    ).astype(jnp.bfloat16)
    packed = jnp.concatenate(
        [keys_after_rotation, projected_value_rows.reshape(token_count, key_heads, HEAD_DIM)], -1
    ).reshape(token_count, key_heads * 2 * HEAD_DIM)
    grouped_query_heads = (
        queries_after_rotation.reshape(token_count, key_heads, queries_per_group, HEAD_DIM)
        .transpose(1, 2, 0, 3)
        .reshape(key_heads, queries_per_group * token_count, HEAD_DIM)
    )
    score_scale = HEAD_DIM ** (-0.5)
    query_total = queries_per_group * token_count
    section = lax.all_gather(packed, "sp", axis=0, tiled=True)
    running_max = jnp.full((key_heads, query_total), far_below, jnp.float32)
    opened = section.reshape(section.shape[0], key_heads, 2 * HEAD_DIM)
    scores = (
        jnp.einsum(
            "hqd,khd->hqk",
            grouped_query_heads,
            opened[:, :, :HEAD_DIM],
            preferred_element_type=jnp.float32,
        )
        * score_scale
    )
    new_peak = jnp.maximum(running_max, jnp.max(scores, -1))
    weights = jnp.exp(scores - new_peak[:, :, None])
    running_sum = jnp.sum(weights, -1)
    running_out = jnp.einsum(
        "hqk,khd->hqd",
        weights.astype(jnp.bfloat16),
        opened[:, :, HEAD_DIM:],
        preferred_element_type=jnp.float32,
    )
    running_max, running_sum, running_out = (new_peak, running_sum, running_out)
    attended = (running_out / running_sum[:, :, None]).astype(jnp.bfloat16)
    attended = (
        attended.reshape(key_heads, queries_per_group, token_count, HEAD_DIM)
        .transpose(2, 0, 1, 3)
        .reshape(token_count, query_heads * HEAD_DIM)
    )
    local_width = residual.shape[1]
    columns = out_weight
    mixed_rows = lax.psum_scatter(
        lax.dot_general(
            columns, attended, (((0,), (1,)), ((), ())), preferred_element_type=jnp.float32
        ).astype(jnp.bfloat16),
        "tp",
        scatter_dimension=0,
        tiled=True,
    ).astype(jnp.float32)
    pre_norm = residual_scale * residual.astype(jnp.float32).T + mixed_rows
    normed = norm_features(pre_norm, norm_gain, D).astype(jnp.bfloat16)
    expert_count = lax.axis_size("sp")
    capacity = 4 * token_count // expert_count
    row_total = expert_count * capacity
    flat_ids = expert_ids.reshape(-1)
    marked = (flat_ids[:, None] == jnp.arange(expert_count, dtype=jnp.int32)[None, :]).astype(
        jnp.int32
    )
    earlier = jnp.cumsum(marked, 0) - marked
    places = (flat_ids * capacity + jnp.sum(earlier * marked, 1)).reshape(token_count, TOPK)
    lane_index = jnp.arange(row_total, dtype=jnp.int32)
    selectors = [
        (places[:, route_rank : route_rank + 1] == lane_index[None, :]).astype(jnp.bfloat16)
        for route_rank in range(TOPK)
    ]
    dispatch = reduce(jnp.add, selectors)
    gate_local = gate_weight[0]
    up_local = up_weight[0]
    down_local = down_weight[0]
    outgoing = lax.dot_general(
        dispatch, normed, (((0,), (1,)), ((), ())), preferred_element_type=jnp.float32
    ).astype(jnp.bfloat16)
    arrived = lax.all_to_all(
        outgoing.reshape(expert_count, capacity, local_width),
        "sp",
        split_axis=0,
        concat_axis=0,
        tiled=True,
    ).reshape(row_total, local_width)
    section = lax.all_gather(arrived, "tp", axis=1, tiled=True)
    gate_sum = jnp.dot(section, gate_local, preferred_element_type=jnp.float32)
    up_sum = jnp.dot(section, up_local, preferred_element_type=jnp.float32)
    hidden = (jax.nn.silu(gate_sum) * up_sum).astype(jnp.bfloat16)
    columns = down_local
    expert_out = lax.psum_scatter(
        lax.dot_general(
            columns, hidden, (((0,), (1,)), ((), ())), preferred_element_type=jnp.float32
        ).astype(jnp.bfloat16),
        "tp",
        scatter_dimension=0,
        tiled=True,
    )
    returned = lax.all_to_all(
        expert_out.reshape(local_width, expert_count, capacity),
        "sp",
        split_axis=1,
        concat_axis=1,
        tiled=True,
    ).reshape(local_width, row_total)
    combined = jnp.zeros((local_width, token_count), jnp.float32)
    for route_rank in range(TOPK):
        chosen = lax.dot_general(
            returned,
            selectors[route_rank],
            (((1,), (1,)), ((), ())),
            preferred_element_type=jnp.float32,
        )
        combined = combined + chosen * route_weights[:, route_rank][None, :]
    second_sum = residual_scale * normed.astype(jnp.float32) + combined
    return norm_features(second_sum, final_gain, D).T.astype(jnp.bfloat16)


def solution(mesh):
    in_specs = (
        P("sp", "tp"),
        P("sp", "tp"),
        P("sp", "tp"),
        P(),
        P(),
        P("sp", "tp"),
        P("tp", None),
        P("tp"),
        P("sp", None),
        P("sp", None),
        P("sp", None, "tp"),
        P("sp", None, "tp"),
        P("sp", "tp", None),
        P("tp"),
    )
    out_specs = P("sp", "tp")
    return jax.shard_map(
        per_device, mesh=mesh, in_specs=in_specs, out_specs=out_specs, check_vma=False
    )
```

profile of v0, /device:TPU:0, one launch (start us, length us, event | category | flops | bytes accessed | tf_op | source)
XLA Modules:
  0.0 209.7 jit_solution(3007069951881743205)
XLA Ops:
  6.6 1.1 copy.42
  7.7 0.7 fusion.43
  8.5 0.1 multiply_cosine_fusion
  8.7 1.0 copy.43
  9.7 0.6 copy-done.2
  10.4 1.0 copy.40
  11.5 0.7 fusion.38
  12.3 40.3 %all-gather.3.cloned.1.call-done = bf16[1024,512]{0,1:T(8,128)(2,1)} async-done(((bf16[128,512]{0,1:T(8,128)(2,1)}), bf16[1024,512]{0,1:T(8,128)(2,1)}) %all-gather.3.cloned.1.call-update) | async-done | bytes 1048592 | tf_op jit(solution)/shard_map/all_gather | solution.py:104
  52.6 2.0 multiply_reduce_fusion
  54.6 0.9 fusion.6
  55.5 0.9 fusion.29
  56.5 1.3 fusion.14
  58.0 0.1 eq.62
  58.1 0.1 eq.58
  58.3 0.6 reduce-window.6
  58.9 0.2 slice_reduce_fusion
  59.2 0.1 reduce_sum.80
  59.5 19.2 %reduce-scatter.3.cloned.1.call-done = bf16[512,128]{0,1:T(8,128)(2,1)} async-done(((bf16[2048,128]{0,1:T(8,128)(2,1)}), bf16[512,128]{0,1:T(8,128)(2,1)}) %reduce-scatter.3.cloned.1.call-update) | async-done | bytes 131088 | tf_op jit(solution)/shard_map/reduce_scatter | solution.py:134
  78.7 1.0 fusion.41
  79.7 5.8 %all-reduce.1 = (f32[128]{0:T(128)S(1)}, f32[128]{0:T(128)S(1)}) all-reduce(f32[128]{0:T(128)S(1)} %get-tuple-element.8, f32[128]{0:T(128)S(1)} %get-tuple-element.7), channel_id=1, replica_groups=mesh['sp'=8,'tp'=4] {'tp'}, use_global_device_ids=true, to_apply=%region_8.9 | all-reduce | flops 256 | bytes 2048 | tf_op jit(solution)/shard_map/psum | solution.py:57
  85.5 1.3 convolution_convert_fusion.1
  86.8 19.8 %all_to_all.10 = bf16[8,64,512]{2,1,0:T(8,128)(2,1)} all-to-all(bf16[8,64,512]{2,1,0:T(8,128)(2,1)S(1)} %bitcast.97), channel_id=1, replica_groups=mesh['sp'=8,'tp'=4] {'sp'}, dimensions={0} | all-to-all | bytes 1048576 | tf_op jit(solution)/shard_map/all_to_all | solution.py:165
  106.7 20.8 %all-gather.5.cloned.1.call-done = bf16[512,2048]{1,0:T(8,128)(2,1)} async-done(((bf16[512,512]{1,0:T(8,128)(2,1)}), bf16[512,2048]{1,0:T(8,128)(2,1)}) %all-gather.5.cloned.1.call-update) | async-done | bytes 2097168 | tf_op jit(solution)/shard_map/all_gather | solution.py:172
  127.5 6.5 %fusion.4 = f32[512,1024]{1,0:T(8,128)} fusion(bf16[512,2048]{1,0:T(8,128)(2,1)} %all-gather.5.cloned.1.call-done, bf16[1,2048,1024]{2,1,0:T(8,128)(2,1)} %param.24), kind=kOutput, calls=%fused_computation.4 | convolution fusion | flops 2147483648 | bytes 8388608 | tf_op jit(solution)/shard_map/dot_general | solution.py:173
  134.0 10.6 %fusion.11 = bf16[2048,512]{0,1:T(8,128)(2,1)} fusion(bf16[1,1024,2048]{2,1,0:T(8,128)(2,1)} %param.26, f32[512,1024]{1,0:T(8,128)} %fusion.4, bf16[512,2048]{1,0:T(8,128)(2,1)} %all-gather.5.cloned.1.call-done, bf16[1,2048,1024]{2,1,0:T(8,128)(2,1)} %param.25), kind=kOutput, calls=%fused_computation.11 | convolution fusion | flops 4299161600 | bytes 14680064 | tf_op jit(solution)/shard_map/dot_general | solution.py:178
  144.6 31.3 %reduce-scatter.5.cloned.1.call-done = bf16[512,512]{0,1:T(8,128)(2,1)} async-done(((bf16[2048,512]{0,1:T(8,128)(2,1)}), bf16[512,512]{0,1:T(8,128)(2,1)}) %reduce-scatter.5.cloned.1.call-update) | async-done | bytes 524304 | tf_op jit(solution)/shard_map/reduce_scatter | solution.py:177
  175.9 5.5 %all-to-all-start.1 = ((bf16[512,8,64]{0,2,1:T(8,128)(2,1)}), bf16[512,8,64]{0,2,1:T(8,128)(2,1)S(1)}, u32[]{:S(2)}, u32[]{:S(2)}) async-start(bf16[512,8,64]{0,2,1:T(8,128)(2,1)} %bitcast.96), calls=%async_computation.3 | async-start | bytes 1048576 | tf_op jit(solution)/shard_map/all_to_all | solution.py:185
  181.5 14.3 %all-to-all-done.1 = bf16[512,8,64]{0,2,1:T(8,128)(2,1)S(1)} async-done(((bf16[512,8,64]{0,2,1:T(8,128)(2,1)}), bf16[512,8,64]{0,2,1:T(8,128)(2,1)S(1)}, u32[]{:S(2)}, u32[]{:S(2)}) %all-to-all-start.1) | async-done | bytes 524320 | tf_op jit(solution)/shard_map/all_to_all | solution.py:185
  195.8 0.3 convolution_multiply_fusion.1
  196.1 0.4 fusion.65
  196.5 5.9 %all-reduce = (f32[128]{0:T(128)S(1)}, f32[128]{0:T(128)S(1)}) all-reduce(f32[128]{0:T(128)S(1)} %get-tuple-element.6, f32[128]{0:T(128)S(1)} %get-tuple-element.5), channel_id=1, replica_groups=mesh['sp'=8,'tp'=4] {'tp'}, use_global_device_ids=true, to_apply=%region_16.17 | all-reduce | flops 256 | bytes 2048 | tf_op jit(solution)/shard_map/psum | solution.py:57
  202.4 0.8 fusion.47
  (50 shorter events, 0.8 us)
Async XLA Ops:
  6.5 50.0 %copy-start = (bf16[512,2048]{1,0:T(8,128)(2,1)S(1)}, bf16[512,2048]{1,0:T(8,128)(2,1)}, u32[]{:S(2)}) copy-start(bf16[512,2048]{1,0:T(8,128)(2,1)} %param.20) | copy-start | bytes 6291460
  6.5 46.1 %all-gather.3.cloned.1.call-start = ((), (), s32[]{:S(2)}) async-start(), calls=%async_computation.4 | async-start | bytes 1179648 | tf_op jit(solution)/shard_map/all_gather | solution.py:104
  9.7 0.7 copy-start.2
  10.3 68.3 %reduce-scatter.3.cloned.1.call-start = ((), (), s32[]{:S(2)}) async-start(), calls=%async_computation.5 | async-start | bytes 655360 | tf_op jit(solution)/shard_map/reduce_scatter | solution.py:134
  52.6 2.9 %copy-start.1 = (bf16[1024,512]{0,1:T(8,128)(2,1)S(1)}, bf16[1024,512]{0,1:T(8,128)(2,1)}, u32[]{:S(2)}) copy-start(bf16[1024,512]{0,1:T(8,128)(2,1)} %all-gather.3.cloned.1.call-done) | copy-start | bytes 3145732
  55.5 2.4 %copy-start.5 = (s32[128,2]{0,1:T(2,128)S(1)}, s32[128,2]{0,1:T(2,128)}, u32[]{:S(2)}) copy-start(s32[128,2]{0,1:T(2,128)} %param.22) | copy-start | bytes 3076
  55.5 23.2 %copy-start.3 = (bf16[128,512]{1,0:T(8,128)(2,1)S(1)}, bf16[128,512]{1,0:T(8,128)(2,1)}, u32[]{:S(2)}) copy-start(bf16[128,512]{1,0:T(8,128)(2,1)} %param.19) | copy-start | bytes 393220
  55.5 30.0 %copy-start.8 = (f32[512]{0:T(512)S(1)}, f32[512]{0:T(512)}, u32[]{:S(2)}) copy-start(f32[512]{0:T(512)} %param.21) | copy-start | bytes 6148
  57.8 69.7 %all-gather.5.cloned.1.call-start = ((), (), s32[]{:S(2)}) async-start(), calls=%async_computation.6 | async-start | bytes 2621440 | tf_op jit(solution)/shard_map/all_gather | solution.py:172
  106.7 69.3 %reduce-scatter.5.cloned.1.call-start = ((), (), s32[]{:S(2)}) async-start(), calls=%async_computation.7 | async-start | bytes 2621440 | tf_op jit(solution)/shard_map/reduce_scatter | solution.py:177
  134.0 47.4 %copy-start.7 = (f32[128,2]{0,1:T(2,128)S(1)}, f32[128,2]{0,1:T(2,128)}, u32[]{:S(2)}) copy-start(f32[128,2]{0,1:T(2,128)} %param.23) | copy-start | bytes 3076
  134.0 62.0 %copy-start.4 = (bf16[512,128]{0,1:T(8,128)(2,1)S(1)}, bf16[512,128]{0,1:T(8,128)(2,1)}, u32[]{:S(2)}) copy-start(bf16[512,128]{0,1:T(8,128)(2,1)} %reduce-scatter.3.cloned.1.call-done) | copy-start | bytes 393220
  144.6 57.8 %copy-start.6 = (f32[512]{0:T(512)S(1)}, f32[512]{0:T(512)}, u32[]{:S(2)}) copy-start(f32[512]{0:T(512)} %param.27) | copy-start | bytes 6148
  175.9 19.8 %all-to-all-start.1 = ((bf16[512,8,64]{0,2,1:T(8,128)(2,1)}), bf16[512,8,64]{0,2,1:T(8,128)(2,1)S(1)}, u32[]{:S(2)}, u32[]{:S(2)}) async-start(bf16[512,8,64]{0,2,1:T(8,128)(2,1)} %bitcast.96), calls=%async_computation.3 | async-start | bytes 1048576 | tf_op jit(solution)/shard_map/all_to_all | solution.py:185
Sparse Core Ops, SparseCore 0:
  10.5 42.1 all-gather.2
  57.9 20.6 reduce-scatter.2
  106.8 20.7 all-gather.4
  144.7 31.1 reduce-scatter.4
where the time goes:
time: 210 us
  waiting for transfers between devices  126 us (60%)
  blocking collectives  31.5 us (15%)
  matrix products  23.2 us (11%)
  between operations  13.4 us (6%)
  starting transfers between devices  5.64 us (3%)
  other arithmetic  5.31 us (3%)
  local copies, waits for them, and re-layouts  4.61 us (2%)
    all_gather x1, waiting for transfers between devices, per_device(): section = lax.all_gather(packed, 'sp', axis=0, tiled=True)  40.3 us
    reduce_scatter x1, waiting for transfers between devices, per_device(): lax.psum_scatter(lax.dot_general(columns, hidden, (((0,), (1,)), ((), ())...  31.3 us
    all_gather x1, waiting for transfers between devices, per_device(): section = lax.all_gather(arrived, 'tp', axis=1, tiled=True)  20.8 us
    all_to_all x1, blocking collectives, per_device(): lax.all_to_all(outgoing.reshape(expert_count, capacity, local_width), 'sp...  19.8 us
    reduce_scatter x1, waiting for transfers between devices, per_device(): lax.psum_scatter(lax.dot_general(columns, attended, (((0,), (1,)), ((), (...  19.2 us
    all_to_all x1, waiting for transfers between devices, per_device(): lax.all_to_all(expert_out.reshape(local_width, expert_count, capacity), '...  14.3 us
    psum x2, blocking collectives, norm_features(): row_sums, squares = lax.psum((row_sums, squares), 'tp')  11.7 us
    dot_general x1, matrix products, per_device(): lax.dot_general(columns, hidden, (((0,), (1,)), ((), ())), preferred_elem...  10.6 us
  transfers between devices with their start and end apart: 5, of which 5 were waited for; matrix products, arithmetic and copies ran while one was open for 2% of the time, Pallas kernels for 0%

commit v1 on v0

--- a/solution.py
+++ b/solution.py
@@ -182,12 +182,17 @@
         scatter_dimension=0,
         tiled=True,
     )
-    returned = lax.all_to_all(
-        expert_out.reshape(local_width, expert_count, capacity),
-        "sp",
-        split_axis=1,
-        concat_axis=1,
-        tiled=True,
+    _balance_ticks = lambda sheet, comm_axis, dim_at, d0: jnp.concatenate(
+        lax.all_to_all(
+            jnp.stack(jnp.split(sheet, lax.axis_size(comm_axis), axis=dim_at), axis=0),
+            comm_axis,
+            0,
+            0,
+        ),
+        d0,
+    )
+    returned = _balance_ticks(
+        expert_out.reshape(local_width, expert_count, capacity), "sp", 1, 1
     ).reshape(local_width, row_total)
     combined = jnp.zeros((local_width, token_count), jnp.float32)
     for route_rank in range(TOPK):

time: 210 us -> 222 us (1.057)
  local copies, waits for them, and re-layouts: 4.61 us -> 16.3 us
    unnamed x22 -> x29, local copies, waits for them, and re-layouts: 3.87 us -> 14.1 us
where the time goes in v1:
time: 222 us; the launch traced here: 221 us
  waiting for transfers between devices  126 us (57%)
  blocking collectives  31.5 us (14%)
  matrix products  23.2 us (10%)
  local copies, waits for them, and re-layouts  16.3 us (7%)
  between operations  13.4 us (6%)
  starting transfers between devices  5.64 us (3%)
  other arithmetic  5.31 us (2%)
    all_gather x1, waiting for transfers between devices, per_device(): section = lax.all_gather(packed, 'sp', axis=0, tiled=True)  40.3 us
    reduce_scatter x1, waiting for transfers between devices, per_device(): lax.psum_scatter(lax.dot_general(columns, hidden, (((0,), (1,)), ((), ())...  31.3 us
    all_gather x1, waiting for transfers between devices, per_device(): section = lax.all_gather(arrived, 'tp', axis=1, tiled=True)  20.8 us
    all_to_all x1, blocking collectives, per_device(): lax.all_to_all(outgoing.reshape(expert_count, capacity, local_width), 'sp...  19.8 us
    reduce_scatter x1, waiting for transfers between devices, per_device(): lax.psum_scatter(lax.dot_general(columns, attended, (((0,), (1,)), ((), (...  19.2 us
    all_to_all x1, waiting for transfers between devices, per_device(): lax.all_to_all(jnp.stack(jnp.split(sheet, lax.axis_size(comm_axis), axis=...  14.3 us
    unnamed x29, local copies, waits for them, and re-layouts  14.1 us
    psum x2, blocking collectives, norm_features(): row_sums, squares = lax.psum((row_sums, squares), 'tp')  11.7 us
  transfers between devices with their start and end apart: 5, of which 5 were waited for; matrix products, arithmetic and copies ran while one was open for 2% of the time, Pallas kernels for 0%

profile of v1, /device:TPU:0, one launch (start us, length us, event | category | flops | bytes accessed | tf_op | source)
XLA Modules:
  0.0 221.4 jit_solution(9057989226252093809)
XLA Ops:
  6.6 1.1 copy.42
  7.7 0.7 fusion.43
  8.7 1.0 copy.43
  9.7 0.6 copy-done.2
  10.4 1.0 copy.40
  11.5 0.7 fusion.38
  12.3 40.3 %all-gather.3.cloned.1.call-done = bf16[1024,512]{0,1:T(8,128)(2,1)} async-done(((bf16[128,512]{0,1:T(8,128)(2,1)}), bf16[1024,512]{0,1:T(8,128)(2,1)}) %all-gather.3.cloned.1.call-update) | async-done | bytes 1048592 | tf_op jit(solution)/shard_map/all_gather | solution.py:104
  52.6 2.0 multiply_reduce_fusion
  54.6 0.9 fusion.6
  55.5 0.9 fusion.29
  56.5 1.3 fusion.14
  59.5 19.2 %reduce-scatter.3.cloned.1.call-done = bf16[512,128]{0,1:T(8,128)(2,1)} async-done(((bf16[2048,128]{0,1:T(8,128)(2,1)}), bf16[512,128]{0,1:T(8,128)(2,1)}) %reduce-scatter.3.cloned.1.call-update) | async-done | bytes 131088 | tf_op jit(solution)/shard_map/reduce_scatter | solution.py:134
  78.7 1.0 fusion.41
  79.7 5.8 %all-reduce.1 = (f32[128]{0:T(128)S(1)}, f32[128]{0:T(128)S(1)}) all-reduce(f32[128]{0:T(128)S(1)} %get-tuple-element.8, f32[128]{0:T(128)S(1)} %get-tuple-element.7), channel_id=1, replica_groups=mesh['sp'=8,'tp'=4] {'tp'}, use_global_device_ids=true, to_apply=%region_8.9 | all-reduce | flops 256 | bytes 2048 | tf_op jit(solution)/shard_map/psum | solution.py:57
  85.5 1.3 convolution_convert_fusion.1
  86.8 19.8 %all_to_all.10 = bf16[8,64,512]{2,1,0:T(8,128)(2,1)} all-to-all(bf16[8,64,512]{2,1,0:T(8,128)(2,1)S(1)} %bitcast.138), channel_id=1, replica_groups=mesh['sp'=8,'tp'=4] {'sp'}, dimensions={0} | all-to-all | bytes 1048576 | tf_op jit(solution)/shard_map/all_to_all | solution.py:165
  106.7 20.8 %all-gather.5.cloned.1.call-done = bf16[512,2048]{1,0:T(8,128)(2,1)} async-done(((bf16[512,512]{1,0:T(8,128)(2,1)}), bf16[512,2048]{1,0:T(8,128)(2,1)}) %all-gather.5.cloned.1.call-update) | async-done | bytes 2097168 | tf_op jit(solution)/shard_map/all_gather | solution.py:172
  127.5 6.5 %fusion.4 = f32[512,1024]{1,0:T(8,128)} fusion(bf16[512,2048]{1,0:T(8,128)(2,1)} %all-gather.5.cloned.1.call-done, bf16[1,2048,1024]{2,1,0:T(8,128)(2,1)} %param.24), kind=kOutput, calls=%fused_computation.4 | convolution fusion | flops 2147483648 | bytes 8388608 | tf_op jit(solution)/shard_map/dot_general | solution.py:173
  134.0 10.5 %fusion.11 = bf16[2048,512]{0,1:T(8,128)(2,1)} fusion(bf16[1,1024,2048]{2,1,0:T(8,128)(2,1)} %param.26, f32[512,1024]{1,0:T(8,128)} %fusion.4, bf16[512,2048]{1,0:T(8,128)(2,1)} %all-gather.5.cloned.1.call-done, bf16[1,2048,1024]{2,1,0:T(8,128)(2,1)} %param.25), kind=kOutput, calls=%fused_computation.11 | convolution fusion | flops 4299161600 | bytes 14680064 | tf_op jit(solution)/shard_map/dot_general | solution.py:178
  144.6 31.3 %reduce-scatter.5.cloned.1.call-done = bf16[512,512]{0,1:T(8,128)(2,1)} async-done(((bf16[2048,512]{0,1:T(8,128)(2,1)}), bf16[512,512]{0,1:T(8,128)(2,1)}) %reduce-scatter.5.cloned.1.call-update) | async-done | bytes 524304 | tf_op jit(solution)/shard_map/reduce_scatter | solution.py:177
  175.9 1.5 fusion.61
  177.4 1.5 fusion.60
  178.8 1.5 fusion.59
  180.3 1.5 fusion.58
  181.8 1.5 fusion.57
  183.2 1.5 fusion.56
  184.7 1.5 fusion.55
  186.2 1.5 fusion.54
  187.6 5.5 %all-to-all-start.1 = ((bf16[8,512,1,64]{1,3,2,0:T(8,128)(2,1)}), bf16[8,512,1,64]{1,3,2,0:T(8,128)(2,1)S(1)}, u32[]{:S(2)}, u32[]{:S(2)}) async-start(bf16[8,512,1,64]{1,3,2,0:T(8,128)(2,1)} %fusion.54), calls=%async_computation.3 | async-start | bytes 1048576 | tf_op jit(solution)/shard_map/all_to_all | solution.py:186
  193.2 14.3 %all-to-all-done.1 = bf16[8,512,1,64]{1,3,2,0:T(8,128)(2,1)S(1)} async-done(((bf16[8,512,1,64]{1,3,2,0:T(8,128)(2,1)}), bf16[8,512,1,64]{1,3,2,0:T(8,128)(2,1)S(1)}, u32[]{:S(2)}, u32[]{:S(2)}) %all-to-all-start.1) | async-done | bytes 524320 | tf_op jit(solution)/shard_map/all_to_all | solution.py:186
  208.1 5.9 %all-reduce = (f32[128]{0:T(128)S(1)}, f32[128]{0:T(128)S(1)}) all-reduce(f32[128]{0:T(128)S(1)} %get-tuple-element.6, f32[128]{0:T(128)S(1)} %get-tuple-element.5), channel_id=1, replica_groups=mesh['sp'=8,'tp'=4] {'tp'}, use_global_device_ids=true, to_apply=%region_16.17 | all-reduce | flops 256 | bytes 2048 | tf_op jit(solution)/shard_map/psum | solution.py:57
  214.1 0.8 fusion.47
  (58 shorter events, 2.9 us)
Async XLA Ops:
  6.5 50.0 %copy-start = (bf16[512,2048]{1,0:T(8,128)(2,1)S(1)}, bf16[512,2048]{1,0:T(8,128)(2,1)}, u32[]{:S(2)}) copy-start(bf16[512,2048]{1,0:T(8,128)(2,1)} %param.20) | copy-start | bytes 6291460
  6.5 46.1 %all-gather.3.cloned.1.call-start = ((), (), s32[]{:S(2)}) async-start(), calls=%async_computation.4 | async-start | bytes 1179648 | tf_op jit(solution)/shard_map/all_gather | solution.py:104
  9.7 0.7 copy-start.2
  10.3 68.3 %reduce-scatter.3.cloned.1.call-start = ((), (), s32[]{:S(2)}) async-start(), calls=%async_computation.5 | async-start | bytes 655360 | tf_op jit(solution)/shard_map/reduce_scatter | solution.py:134
  52.6 2.9 %copy-start.1 = (bf16[1024,512]{0,1:T(8,128)(2,1)S(1)}, bf16[1024,512]{0,1:T(8,128)(2,1)}, u32[]{:S(2)}) copy-start(bf16[1024,512]{0,1:T(8,128)(2,1)} %all-gather.3.cloned.1.call-done) | copy-start | bytes 3145732
  55.5 2.4 %copy-start.5 = (s32[128,2]{0,1:T(2,128)S(1)}, s32[128,2]{0,1:T(2,128)}, u32[]{:S(2)}) copy-start(s32[128,2]{0,1:T(2,128)} %param.22) | copy-start | bytes 3076
  55.5 23.2 %copy-start.3 = (bf16[128,512]{1,0:T(8,128)(2,1)S(1)}, bf16[128,512]{1,0:T(8,128)(2,1)}, u32[]{:S(2)}) copy-start(bf16[128,512]{1,0:T(8,128)(2,1)} %param.19) | copy-start | bytes 393220
  55.5 30.0 %copy-start.8 = (f32[512]{0:T(512)S(1)}, f32[512]{0:T(512)}, u32[]{:S(2)}) copy-start(f32[512]{0:T(512)} %param.21) | copy-start | bytes 6148
  57.8 69.7 %all-gather.5.cloned.1.call-start = ((), (), s32[]{:S(2)}) async-start(), calls=%async_computation.6 | async-start | bytes 2621440 | tf_op jit(solution)/shard_map/all_gather | solution.py:172
  106.7 69.3 %reduce-scatter.5.cloned.1.call-start = ((), (), s32[]{:S(2)}) async-start(), calls=%async_computation.7 | async-start | bytes 2621440 | tf_op jit(solution)/shard_map/reduce_scatter | solution.py:177
  144.6 48.6 %copy-start.7 = (f32[128,2]{0,1:T(2,128)S(1)}, f32[128,2]{0,1:T(2,128)}, u32[]{:S(2)}) copy-start(f32[128,2]{0,1:T(2,128)} %param.23) | copy-start | bytes 3076
  144.6 63.2 %copy-start.4 = (bf16[512,128]{0,1:T(8,128)(2,1)S(1)}, bf16[512,128]{0,1:T(8,128)(2,1)}, u32[]{:S(2)}) copy-start(bf16[512,128]{0,1:T(8,128)(2,1)} %reduce-scatter.3.cloned.1.call-done) | copy-start | bytes 393220
  144.6 69.5 %copy-start.6 = (f32[512]{0:T(512)S(1)}, f32[512]{0:T(512)}, u32[]{:S(2)}) copy-start(f32[512]{0:T(512)} %param.27) | copy-start | bytes 6148
  187.6 19.8 %all-to-all-start.1 = ((bf16[8,512,1,64]{1,3,2,0:T(8,128)(2,1)}), bf16[8,512,1,64]{1,3,2,0:T(8,128)(2,1)S(1)}, u32[]{:S(2)}, u32[]{:S(2)}) async-start(bf16[8,512,1,64]{1,3,2,0:T(8,128)(2,1)} %fusion.54), calls=%async_computation.3 | async-start | bytes 1048576 | tf_op jit(solution)/shard_map/all_to_all | solution.py:186
Sparse Core Ops, SparseCore 0:
  10.5 42.1 all-gather.2
  57.9 20.6 reduce-scatter.2
  106.8 20.7 all-gather.4
  144.7 31.1 reduce-scatter.4
